TPU v7x, 256 devices: a whole 4x4x8 slice. The times are simulated.
256 devices in a mesh: sp: 32 (over z, x), tp: 8 (over y, core).
Axes of the slice: x: 4, y: 4, z: 8, core: 2. Of those that a mesh axis runs over, the one named last changes fastest.
Arguments:
- tokens: bfloat16 [16384, 2048], P(('sp', 'tp')), may hold values from -40 to 40
- query_weight: bfloat16 [2048, 1024], P(None, 'tp'), may hold values from -0.1875 to 0.1875
- key_weight: bfloat16 [2048, 256], replicated, may hold values from -0.1875 to 0.1875
- value_weight: bfloat16 [2048, 256], replicated, may hold values from -0.125 to 0.125
- out_weight: bfloat16 [1024, 2048], replicated, may hold values from -0.1875 to 0.1875
- head_gain: float32 [128], replicated, may hold values from 0.1 to 1.9
- lambdas: float32 [8], P('tp'), may hold values from 0.3 to 0.8
Outputs:
- mixed: bfloat16 [16384, 2048], P(('sp', 'tp'))
All inputs are finite; a program needn't handle non-finite values.
Results may differ from a plain program's by a relative error of at most 0.018.
The roundings to bfloat16 on the way count: a program that leaves them out, or rounds other values in their place, can miss the bound.
Values may be sent and summed in bfloat16 or wider, within the bound.
No kernel may reach another device: no remote copies, remote signals or barrier semaphores. Data moves between devices by JAX's collectives and lax.ppermute only.
A program may use at most 64 MiB of HBM per device.

v0:
```python
import jax
import jax.numpy as jnp
from jax import lax
from jax.sharding import PartitionSpec as P

H = 8
DH = 64
DV = 128
epsilon = 1e-06
rope_base = 10000.0
fold_span = 2048


def joined_along(parts, dim):
    parts = jnp.moveaxis(parts, 0, dim)
    shape = parts.shape
    return parts.reshape(*shape[:dim], shape[dim] * shape[dim + 1], *shape[dim + 2 :])


def copy_for_each(x, axis):
    count = lax.axis_size(axis)
    return lax.all_to_all(jnp.broadcast_to(x[None], (count, *x.shape)), axis, 0, 0, tiled=True)


def gather_directly(x, axis, dim):
    return joined_along(copy_for_each(x, axis), dim)


def sent_together(arrays, axis, dim, along):
    ends, at = ([], 0)
    for a in arrays[:-1]:
        at += a.shape[along]
        ends.append(at)
    both = jnp.concatenate(arrays, axis=along)
    return tuple(jnp.split(lax.all_gather(both, axis, axis=dim, tiled=True), ends, axis=along))


def rotate(tensor_in, places):
    head_dim = tensor_in.shape[-1]
    half_dim = head_dim // 2
    frequency = rope_base ** (-(jnp.arange(half_dim, dtype=jnp.float32) * 2.0) / head_dim)
    angles = places[:, None] * frequency[None, :]
    angles = angles.reshape((places.shape[0],) + (1,) * (tensor_in.ndim - 2) + (half_dim,))
    cosine = jnp.cos(angles)
    sine_part = jnp.sin(angles)
    first = tensor_in[..., :half_dim]
    second = tensor_in[..., half_dim:]
    return jnp.concatenate(
        [first * cosine - second * sine_part, first * sine_part + second * cosine], axis=-1
    )


def local(tokens, query_weight, key_weight, value_weight, out_weight, head_gain, lambdas):
    heads_dev = query_weight.shape[1] // (2 * DH)
    kv_heads = key_weight.shape[1] // (2 * DH)
    group_size = H // kv_heads
    kv_index = lax.axis_index("tp") * heads_dev // group_size
    key_cols = lax.dynamic_slice_in_dim(key_weight, kv_index * (2 * DH), 2 * DH, 1)
    value_cols = lax.dynamic_slice_in_dim(value_weight, kv_index * DV, DV, 1)
    stacked = jnp.concatenate([query_weight, key_cols, value_cols], axis=1)
    projected = jnp.dot(
        gather_directly(tokens, "tp", 0), stacked, preferred_element_type=jnp.float32
    )
    seq_rows = projected.shape[0]
    places = (lax.axis_index("sp") * seq_rows + jnp.arange(seq_rows, dtype=jnp.int32)).astype(
        jnp.float32
    )
    query_cols = heads_dev * 2 * DH
    queries = rotate(projected[:, :query_cols].reshape(seq_rows, heads_dev, 2, DH), places).astype(
        jnp.bfloat16
    )
    key_rows = rotate(
        projected[:, query_cols : query_cols + 2 * DH].reshape(seq_rows, 2, DH), places
    )
    key_rows = key_rows.astype(jnp.bfloat16).reshape(seq_rows, 2 * DH)
    value_rows = projected[:, query_cols + 2 * DH :].astype(jnp.bfloat16)
    score_scale = DH ** (-0.5)

    def update(carried, key_block, value_block):
        running_max, running_sum, weighted = carried
        scores = (
            jnp.einsum(
                "qhcd,kcd->cqhk",
                queries,
                key_block.reshape(key_block.shape[0], 2, DH),
                preferred_element_type=jnp.float32,
            )
            * score_scale
        )
        new_max = jnp.maximum(running_max, jnp.max(scores, axis=-1))
        weights = jnp.exp(scores - new_max[..., None])
        shrink = jnp.exp(running_max - new_max)
        running_sum = shrink * running_sum + jnp.sum(weights, axis=-1)
        weighted = shrink[..., None] * weighted + jnp.einsum(
            "cqhk,kv->cqhv",
            weights.astype(jnp.bfloat16),
            value_block,
            preferred_element_type=jnp.float32,
        )
        return (new_max, running_sum, weighted)

    initial = (
        jnp.full((2, seq_rows, heads_dev), -1e30, jnp.float32),
        jnp.zeros((2, seq_rows, heads_dev), jnp.float32),
        jnp.zeros((2, seq_rows, heads_dev, DV), jnp.float32),
    )
    key_piece, value_piece = sent_together((key_rows, value_rows), "sp", 0, 1)
    row_count = key_piece.shape[0]

    def one_span(state_now, span_index):
        key_block = lax.dynamic_slice_in_dim(key_piece, span_index * fold_span, fold_span, 0)
        value_block = lax.dynamic_slice_in_dim(value_piece, span_index * fold_span, fold_span, 0)
        return (update(state_now, key_block, value_block), None)

    running_max, running_sum, weighted = lax.scan(
        one_span, initial, jnp.arange(row_count // fold_span, dtype=jnp.int32)
    )[0]
    attended = (
        weighted[0] / running_sum[0][..., None]
        - lambdas[None, :, None] * weighted[1] / running_sum[1][..., None]
    )
    mean_square = jnp.mean(attended * attended, axis=-1, keepdims=True)
    normed = (attended * lax.rsqrt(mean_square + epsilon) * head_gain).astype(jnp.bfloat16)
    normed = normed.reshape(seq_rows, heads_dev * DV)
    regrouped = lax.all_to_all(normed, "tp", split_axis=0, concat_axis=1, tiled=True)
    return jnp.dot(regrouped, out_weight, preferred_element_type=jnp.float32).astype(jnp.bfloat16)


def solution(mesh):
    return jax.shard_map(
        local,
        mesh=mesh,
        in_specs=(P(("sp", "tp"), None), P(None, "tp"), P(), P(), P(), P(), P("tp")),
        out_specs=P(("sp", "tp"), None),
        check_vma=False,
    )
```

profile of v0, /device:TPU:1, one launch (start us, length us, event | category | flops | bytes accessed | tf_op | source)
XLA Modules:
  0.0 288.7 jit_solution(8956814849785031514)
XLA Ops:
  6.5 2.5 broadcast_in_dim.11
  9.1 6.7 %all-to-all-start = ((bf16[8,64,2048]{2,1,0:T(8,128)(2,1)}), bf16[8,64,2048]{2,1,0:T(8,128)(2,1)S(1)}, u32[]{:S(2)}, u32[]{:S(2)}) async-start(bf16[8,64,2048]{2,1,0:T(8,128)(2,1)} %broadcast_in_dim.11), calls=%async_computation | async-start | bytes 4194304 | tf_op jit(solution)/shard_map/all_to_all | solution.py:22
  15.8 0.3 multiply_cosine_fusion
  16.1 1.3 constant_dynamic-slice_fusion.1
  17.4 24.6 %all-to-all-done = bf16[8,64,2048]{2,1,0:T(8,128)(2,1)S(1)} async-done(((bf16[8,64,2048]{2,1,0:T(8,128)(2,1)}), bf16[8,64,2048]{2,1,0:T(8,128)(2,1)S(1)}, u32[]{:S(2)}, u32[]{:S(2)}) %all-to-all-start) | async-done | bytes 2097184 | tf_op jit(solution)/shard_map/all_to_all | solution.py:22
  42.0 2.1 fusion.24
  44.2 0.7 pad_maximum_fusion
  45.7 98.9 %all-gather.2.cloned.1.call-done = bf16[16384,256]{0,1:T(8,128)(2,1)} async-done(((bf16[512,256]{0,1:T(8,128)(2,1)}), bf16[16384,256]{0,1:T(8,128)(2,1)}) %all-gather.2.cloned.1.call-update) | async-done | bytes 8388624 | tf_op jit(solution)/shard_map/all_gather | solution.py:35
  144.6 5.8 %fusion.33 = (bf16[16384,128]{0,1:T(8,128)(2,1)}, bf16[16384,128]{0,1:T(8,128)(2,1)}) fusion(bf16[16384,256]{0,1:T(8,128)(2,1)} %all-gather.2.cloned.1.call-done), kind=kLoop, calls=%fused_computation.57 | loop fusion | bytes 16777216 | tf_op jit(solution)/shard_map/split | solution.py:35
  150.4 113.6 %while.15 = (s32[]{:T(128)}, f32[2,512,1]{1,0,2:T(2,128)S(1)}, f32[2,512,1]{1,0,2:T(2,128)S(1)}, f32[2,512,1,128]{3,1,0,2:T(8,128)S(1)}, s32[8]{0:T(128)S(1)}, /...) while((s32[]{:T(128)}, f32[2,512,1]{1,0,2:T(2,128)S(1)}, ...), condition=%wide.region_3.4_spmd.clone, body=%wide.region_0.3_spmd.clone.sunk | while | flops 822482944 | bytes 62062812 | solution.py:115
  150.4 0.6 dynamic_slice.33
  151.7 1.1 constant_dynamic-slice_fusion.4
  152.8 4.5 %bitcast_reduce_fusion.2 = (f32[2,512]{1,0:T(2,128)S(1)}, f32[2,2048,512]{2,1,0:T(8,128)}) fusion(bf16[2048,2,64]{0,2,1:T(8,128)(2,1)S(1)} %bitcast.99, bf16[512,1,2,64]{0,3,2,1:T(8,128)(2,1)S(1)} %get-tuple-element.234), kind=kOutput, calls=%fused_computation.1.clone.1 | convolution fusion | flops 272628736 | bytes 9048064 | tf_op jit(solution)/shard_map/while/body/eval_jaxpr/qhcd,kcd->cqhk/dot_general | solution.py:82
  157.3 5.3 %fusion.50 = f32[2,512,1,128]{3,1,0,2:T(8,128)S(1)} fusion(f32[2,2048,512]{2,1,0:T(8,128)} %get-tuple-element.202, f32[2,512]{1,0:T(2,128)S(1)} %bitcast.102, f32[2,512,1,128]{3,1,0,2:T(8,128)S(1)} %get-tuple-element.219, bf16[16384,128]{0,1:T(8,128)(2,1)} %get-tuple-element.235, s32[]{:T(128)S(6)} %select_n.17, ...), kind=kOutput, calls=%fused_computation.7.clone.1 | convolution fusion | flops 543555584 | bytes 9969669 | tf_op jit(solution)/shard_map/while/body/eval_jaxpr/cqhk,kv->cqhv/dot_general | solution.py:94
  162.6 0.6 copy-done
  163.2 1.4 fusion.49
  164.6 0.6 dynamic_slice.33
  165.9 1.1 constant_dynamic-slice_fusion.4
  167.0 4.5 %bitcast_reduce_fusion.2 = (f32[2,512]{1,0:T(2,128)S(1)}, f32[2,2048,512]{2,1,0:T(8,128)}) fusion(bf16[2048,2,64]{0,2,1:T(8,128)(2,1)S(1)} %bitcast.99, bf16[512,1,2,64]{0,3,2,1:T(8,128)(2,1)S(1)} %get-tuple-element.234), kind=kOutput, calls=%fused_computation.1.clone.1 | convolution fusion | flops 272628736 | bytes 9048064 | tf_op jit(solution)/shard_map/while/body/eval_jaxpr/qhcd,kcd->cqhk/dot_general | solution.py:82
  171.5 5.3 %fusion.50 = f32[2,512,1,128]{3,1,0,2:T(8,128)S(1)} fusion(f32[2,2048,512]{2,1,0:T(8,128)} %get-tuple-element.202, f32[2,512]{1,0:T(2,128)S(1)} %bitcast.102, f32[2,512,1,128]{3,1,0,2:T(8,128)S(1)} %get-tuple-element.219, bf16[16384,128]{0,1:T(8,128)(2,1)} %get-tuple-element.235, s32[]{:T(128)S(6)} %select_n.17, ...), kind=kOutput, calls=%fused_computation.7.clone.1 | convolution fusion | flops 543555584 | bytes 9969669 | tf_op jit(solution)/shard_map/while/body/eval_jaxpr/cqhk,kv->cqhv/dot_general | solution.py:94
  176.8 0.6 copy-done
  177.4 1.4 fusion.49
  178.8 0.6 dynamic_slice.33
  180.1 1.1 constant_dynamic-slice_fusion.4
  181.2 4.5 %bitcast_reduce_fusion.2 = (f32[2,512]{1,0:T(2,128)S(1)}, f32[2,2048,512]{2,1,0:T(8,128)}) fusion(bf16[2048,2,64]{0,2,1:T(8,128)(2,1)S(1)} %bitcast.99, bf16[512,1,2,64]{0,3,2,1:T(8,128)(2,1)S(1)} %get-tuple-element.234), kind=kOutput, calls=%fused_computation.1.clone.1 | convolution fusion | flops 272628736 | bytes 9048064 | tf_op jit(solution)/shard_map/while/body/eval_jaxpr/qhcd,kcd->cqhk/dot_general | solution.py:82
  185.7 5.3 %fusion.50 = f32[2,512,1,128]{3,1,0,2:T(8,128)S(1)} fusion(f32[2,2048,512]{2,1,0:T(8,128)} %get-tuple-element.202, f32[2,512]{1,0:T(2,128)S(1)} %bitcast.102, f32[2,512,1,128]{3,1,0,2:T(8,128)S(1)} %get-tuple-element.219, bf16[16384,128]{0,1:T(8,128)(2,1)} %get-tuple-element.235, s32[]{:T(128)S(6)} %select_n.17, ...), kind=kOutput, calls=%fused_computation.7.clone.1 | convolution fusion | flops 543555584 | bytes 9969669 | tf_op jit(solution)/shard_map/while/body/eval_jaxpr/cqhk,kv->cqhv/dot_general | solution.py:94
  191.0 0.6 copy-done
  191.6 1.4 fusion.49
  193.0 0.6 dynamic_slice.33
  194.3 1.1 constant_dynamic-slice_fusion.4
  195.4 4.5 %bitcast_reduce_fusion.2 = (f32[2,512]{1,0:T(2,128)S(1)}, f32[2,2048,512]{2,1,0:T(8,128)}) fusion(bf16[2048,2,64]{0,2,1:T(8,128)(2,1)S(1)} %bitcast.99, bf16[512,1,2,64]{0,3,2,1:T(8,128)(2,1)S(1)} %get-tuple-element.234), kind=kOutput, calls=%fused_computation.1.clone.1 | convolution fusion | flops 272628736 | bytes 9048064 | tf_op jit(solution)/shard_map/while/body/eval_jaxpr/qhcd,kcd->cqhk/dot_general | solution.py:82
  199.9 5.3 %fusion.50 = f32[2,512,1,128]{3,1,0,2:T(8,128)S(1)} fusion(f32[2,2048,512]{2,1,0:T(8,128)} %get-tuple-element.202, f32[2,512]{1,0:T(2,128)S(1)} %bitcast.102, f32[2,512,1,128]{3,1,0,2:T(8,128)S(1)} %get-tuple-element.219, bf16[16384,128]{0,1:T(8,128)(2,1)} %get-tuple-element.235, s32[]{:T(128)S(6)} %select_n.17, ...), kind=kOutput, calls=%fused_computation.7.clone.1 | convolution fusion | flops 543555584 | bytes 9969669 | tf_op jit(solution)/shard_map/while/body/eval_jaxpr/cqhk,kv->cqhv/dot_general | solution.py:94
  205.2 0.6 copy-done
  205.8 1.4 fusion.49
  207.2 0.6 dynamic_slice.33
  208.5 1.1 constant_dynamic-slice_fusion.4
  209.6 4.5 %bitcast_reduce_fusion.2 = (f32[2,512]{1,0:T(2,128)S(1)}, f32[2,2048,512]{2,1,0:T(8,128)}) fusion(bf16[2048,2,64]{0,2,1:T(8,128)(2,1)S(1)} %bitcast.99, bf16[512,1,2,64]{0,3,2,1:T(8,128)(2,1)S(1)} %get-tuple-element.234), kind=kOutput, calls=%fused_computation.1.clone.1 | convolution fusion | flops 272628736 | bytes 9048064 | tf_op jit(solution)/shard_map/while/body/eval_jaxpr/qhcd,kcd->cqhk/dot_general | solution.py:82
  214.1 5.3 %fusion.50 = f32[2,512,1,128]{3,1,0,2:T(8,128)S(1)} fusion(f32[2,2048,512]{2,1,0:T(8,128)} %get-tuple-element.202, f32[2,512]{1,0:T(2,128)S(1)} %bitcast.102, f32[2,512,1,128]{3,1,0,2:T(8,128)S(1)} %get-tuple-element.219, bf16[16384,128]{0,1:T(8,128)(2,1)} %get-tuple-element.235, s32[]{:T(128)S(6)} %select_n.17, ...), kind=kOutput, calls=%fused_computation.7.clone.1 | convolution fusion | flops 543555584 | bytes 9969669 | tf_op jit(solution)/shard_map/while/body/eval_jaxpr/cqhk,kv->cqhv/dot_general | solution.py:94
  219.4 0.6 copy-done
  220.0 1.4 fusion.49
  221.4 0.6 dynamic_slice.33
  222.7 1.1 constant_dynamic-slice_fusion.4
  223.8 4.5 %bitcast_reduce_fusion.2 = (f32[2,512]{1,0:T(2,128)S(1)}, f32[2,2048,512]{2,1,0:T(8,128)}) fusion(bf16[2048,2,64]{0,2,1:T(8,128)(2,1)S(1)} %bitcast.99, bf16[512,1,2,64]{0,3,2,1:T(8,128)(2,1)S(1)} %get-tuple-element.234), kind=kOutput, calls=%fused_computation.1.clone.1 | convolution fusion | flops 272628736 | bytes 9048064 | tf_op jit(solution)/shard_map/while/body/eval_jaxpr/qhcd,kcd->cqhk/dot_general | solution.py:82
  228.3 5.3 %fusion.50 = f32[2,512,1,128]{3,1,0,2:T(8,128)S(1)} fusion(f32[2,2048,512]{2,1,0:T(8,128)} %get-tuple-element.202, f32[2,512]{1,0:T(2,128)S(1)} %bitcast.102, f32[2,512,1,128]{3,1,0,2:T(8,128)S(1)} %get-tuple-element.219, bf16[16384,128]{0,1:T(8,128)(2,1)} %get-tuple-element.235, s32[]{:T(128)S(6)} %select_n.17, ...), kind=kOutput, calls=%fused_computation.7.clone.1 | convolution fusion | flops 543555584 | bytes 9969669 | tf_op jit(solution)/shard_map/while/body/eval_jaxpr/cqhk,kv->cqhv/dot_general | solution.py:94
  233.6 0.6 copy-done
  234.2 1.4 fusion.49
  235.6 0.6 dynamic_slice.33
  236.9 1.1 constant_dynamic-slice_fusion.4
  238.0 4.5 %bitcast_reduce_fusion.2 = (f32[2,512]{1,0:T(2,128)S(1)}, f32[2,2048,512]{2,1,0:T(8,128)}) fusion(bf16[2048,2,64]{0,2,1:T(8,128)(2,1)S(1)} %bitcast.99, bf16[512,1,2,64]{0,3,2,1:T(8,128)(2,1)S(1)} %get-tuple-element.234), kind=kOutput, calls=%fused_computation.1.clone.1 | convolution fusion | flops 272628736 | bytes 9048064 | tf_op jit(solution)/shard_map/while/body/eval_jaxpr/qhcd,kcd->cqhk/dot_general | solution.py:82
  242.5 5.3 %fusion.50 = f32[2,512,1,128]{3,1,0,2:T(8,128)S(1)} fusion(f32[2,2048,512]{2,1,0:T(8,128)} %get-tuple-element.202, f32[2,512]{1,0:T(2,128)S(1)} %bitcast.102, f32[2,512,1,128]{3,1,0,2:T(8,128)S(1)} %get-tuple-element.219, bf16[16384,128]{0,1:T(8,128)(2,1)} %get-tuple-element.235, s32[]{:T(128)S(6)} %select_n.17, ...), kind=kOutput, calls=%fused_computation.7.clone.1 | convolution fusion | flops 543555584 | bytes 9969669 | tf_op jit(solution)/shard_map/while/body/eval_jaxpr/cqhk,kv->cqhv/dot_general | solution.py:94
  247.8 0.6 copy-done
  248.4 1.4 fusion.49
  249.8 0.6 dynamic_slice.33
  251.1 1.1 constant_dynamic-slice_fusion.4
  252.2 4.5 %bitcast_reduce_fusion.2 = (f32[2,512]{1,0:T(2,128)S(1)}, f32[2,2048,512]{2,1,0:T(8,128)}) fusion(bf16[2048,2,64]{0,2,1:T(8,128)(2,1)S(1)} %bitcast.99, bf16[512,1,2,64]{0,3,2,1:T(8,128)(2,1)S(1)} %get-tuple-element.234), kind=kOutput, calls=%fused_computation.1.clone.1 | convolution fusion | flops 272628736 | bytes 9048064 | tf_op jit(solution)/shard_map/while/body/eval_jaxpr/qhcd,kcd->cqhk/dot_general | solution.py:82
  256.7 5.3 %fusion.50 = f32[2,512,1,128]{3,1,0,2:T(8,128)S(1)} fusion(f32[2,2048,512]{2,1,0:T(8,128)} %get-tuple-element.202, f32[2,512]{1,0:T(2,128)S(1)} %bitcast.102, f32[2,512,1,128]{3,1,0,2:T(8,128)S(1)} %get-tuple-element.219, bf16[16384,128]{0,1:T(8,128)(2,1)} %get-tuple-element.235, s32[]{:T(128)S(6)} %select_n.17, ...), kind=kOutput, calls=%fused_computation.7.clone.1 | convolution fusion | flops 543555584 | bytes 9969669 | tf_op jit(solution)/shard_map/while/body/eval_jaxpr/cqhk,kv->cqhv/dot_general | solution.py:94
  262.0 0.6 copy-done
  262.6 1.4 fusion.49
  264.1 0.3 fusion.29
  264.4 0.1 rsqrt.12
  264.5 0.1 div.76
  264.6 0.3 multiply_convert_fusion
  264.9 13.2 %all_to_all.21 = bf16[8,64,128]{2,1,0:T(8,128)(2,1)S(1)} all-to-all(bf16[8,64,128]{2,1,0:T(8,128)(2,1)S(1)} %multiply_convert_fusion), channel_id=1, replica_groups=mesh['sp'=32,'tp'=8] {'tp'}, dimensions={0} | all-to-all | bytes 262144 | tf_op jit(solution)/shard_map/all_to_all | solution.py:125
  278.1 3.7 %convolution_convert_fusion = bf16[64,2048]{1,0:T(8,128)(2,1)} fusion(bf16[1024,2048]{1,0:T(8,128)(2,1)} %param.13, bf16[8,64,128]{2,1,0:T(8,128)(2,1)S(1)} %all_to_all.21), kind=kOutput, calls=%fused_computation.22 | convolution fusion | flops 268566528 | bytes 4587520 | tf_op jit(solution)/shard_map/dot_general | solution.py:126
  (52 shorter events, 0.6 us)
Async XLA Ops:
  9.1 32.9 %all-to-all-start = ((bf16[8,64,2048]{2,1,0:T(8,128)(2,1)}), bf16[8,64,2048]{2,1,0:T(8,128)(2,1)S(1)}, u32[]{:S(2)}, u32[]{:S(2)}) async-start(bf16[8,64,2048]{2,1,0:T(8,128)(2,1)} %broadcast_in_dim.11), calls=%async_computation | async-start | bytes 4194304 | tf_op jit(solution)/shard_map/all_to_all | solution.py:22
  15.8 128.8 %all-gather.2.cloned.1.call-start = ((), (), s32[]{:S(2)}) async-start(), calls=%async_computation.2 | async-start | bytes 8650752 | tf_op jit(solution)/shard_map/all_gather | solution.py:35
  150.4 114.2 %copy-start.1 = (f32[128]{0:T(128)S(1)}, f32[128]{0:T(128)}, u32[]{:S(2)}) copy-start(f32[128]{0:T(128)} %param.14) | copy-start | bytes 1540
  157.3 5.9 %copy-start = (f32[2,2048,512]{2,1,0:T(8,128)S(1)}, f32[2,2048,512]{2,1,0:T(8,128)}, u32[]{:S(2)}) copy-start(f32[2,2048,512]{2,1,0:T(8,128)} %get-tuple-element.202) | copy-start | bytes 25165828 | tf_op jit(solution)/shard_map/while
  171.5 5.9 %copy-start = (f32[2,2048,512]{2,1,0:T(8,128)S(1)}, f32[2,2048,512]{2,1,0:T(8,128)}, u32[]{:S(2)}) copy-start(f32[2,2048,512]{2,1,0:T(8,128)} %get-tuple-element.202) | copy-start | bytes 25165828 | tf_op jit(solution)/shard_map/while
  185.7 5.9 %copy-start = (f32[2,2048,512]{2,1,0:T(8,128)S(1)}, f32[2,2048,512]{2,1,0:T(8,128)}, u32[]{:S(2)}) copy-start(f32[2,2048,512]{2,1,0:T(8,128)} %get-tuple-element.202) | copy-start | bytes 25165828 | tf_op jit(solution)/shard_map/while
  199.9 5.9 %copy-start = (f32[2,2048,512]{2,1,0:T(8,128)S(1)}, f32[2,2048,512]{2,1,0:T(8,128)}, u32[]{:S(2)}) copy-start(f32[2,2048,512]{2,1,0:T(8,128)} %get-tuple-element.202) | copy-start | bytes 25165828 | tf_op jit(solution)/shard_map/while
  214.1 5.9 %copy-start = (f32[2,2048,512]{2,1,0:T(8,128)S(1)}, f32[2,2048,512]{2,1,0:T(8,128)}, u32[]{:S(2)}) copy-start(f32[2,2048,512]{2,1,0:T(8,128)} %get-tuple-element.202) | copy-start | bytes 25165828 | tf_op jit(solution)/shard_map/while
  228.3 5.9 %copy-start = (f32[2,2048,512]{2,1,0:T(8,128)S(1)}, f32[2,2048,512]{2,1,0:T(8,128)}, u32[]{:S(2)}) copy-start(f32[2,2048,512]{2,1,0:T(8,128)} %get-tuple-element.202) | copy-start | bytes 25165828 | tf_op jit(solution)/shard_map/while
  242.5 5.9 %copy-start = (f32[2,2048,512]{2,1,0:T(8,128)S(1)}, f32[2,2048,512]{2,1,0:T(8,128)}, u32[]{:S(2)}) copy-start(f32[2,2048,512]{2,1,0:T(8,128)} %get-tuple-element.202) | copy-start | bytes 25165828 | tf_op jit(solution)/shard_map/while
  256.7 5.9 %copy-start = (f32[2,2048,512]{2,1,0:T(8,128)S(1)}, f32[2,2048,512]{2,1,0:T(8,128)}, u32[]{:S(2)}) copy-start(f32[2,2048,512]{2,1,0:T(8,128)} %get-tuple-element.202) | copy-start | bytes 25165828 | tf_op jit(solution)/shard_map/while
Sparse Core Ops, SparseCore 0:
  45.1 99.4 all-gather.1
where the time goes:
time: 289 us
  waiting for transfers between devices  124 us (43%)
  matrix products  84.1 us (29%)
  local copies, waits for them, and re-layouts  28.4 us (10%)
  between operations  14.2 us (5%)
  blocking collectives  13.2 us (5%)
  other arithmetic  13 us (4%)
  starting transfers between devices  6.71 us (2%)
  loops' own time  5.6 us (2%)
    all_gather x1, waiting for transfers between devices, sent_together(): lax.all_gather(both, axis, axis=dim, tiled=True)  98.9 us
    dot_general x8, matrix products, update(): jnp.einsum('cqhk,kv->cqhv', weights.astype(jnp.bfloat16), value_block, pr...  42.1 us
    dot_general x8, matrix products, update(): jnp.einsum('qhcd,kcd->cqhk', queries, key_block.reshape(key_block.shape[0...  36.2 us
    all_to_all x1, waiting for transfers between devices, copy_for_each(): lax.all_to_all(jnp.broadcast_to(x[None], (count, *x.shape)), axis, 0, 0,...  24.6 us
    all_to_all x1, blocking collectives, local(): lax.all_to_all(normed, 'tp', split_axis=0, concat_axis=1, tiled=True)  13.2 us
    reduce_sum x8, other arithmetic, update(): running_sum = shrink * running_sum + jnp.sum(weights, axis=-1)  11 us
    dynamic_slice x8, local copies, waits for them, and re-layouts, one_span(): lax.dynamic_slice_in_dim(key_piece, span_index * fold_span, fold_span, 0)  8.65 us
    all_to_all x1, starting transfers between devices, copy_for_each(): lax.all_to_all(jnp.broadcast_to(x[None], (count, *x.shape)), axis, 0, 0,...  6.7 us
  transfers between devices with their start and end apart: 2, of which 2 were waited for; matrix products, arithmetic and copies ran while one was open for 1% of the time, Pallas kernels for 0%

commit v1 on v0

--- a/solution.py
+++ b/solution.py
@@ -122,7 +122,10 @@
     mean_square = jnp.mean(attended * attended, axis=-1, keepdims=True)
     normed = (attended * lax.rsqrt(mean_square + epsilon) * head_gain).astype(jnp.bfloat16)
     normed = normed.reshape(seq_rows, heads_dev * DV)
-    regrouped = lax.all_to_all(normed, "tp", split_axis=0, concat_axis=1, tiled=True)
+    regrouped = jnp.concatenate(
+        lax.all_to_all(jnp.stack(jnp.split(normed, lax.axis_size("tp"), axis=0)), "tp", 0, 0),
+        axis=1,
+    )
     return jnp.dot(regrouped, out_weight, preferred_element_type=jnp.float32).astype(jnp.bfloat16)
 
 

time: 289 us -> 289 us (level)
  no operation moved by 1% of the time
where the time goes in v1:
time: 289 us; the launch traced here: 288 us
  waiting for transfers between devices  124 us (43%)
  matrix products  84.1 us (29%)
  local copies, waits for them, and re-layouts  28.2 us (10%)
  between operations  14.2 us (5%)
  blocking collectives  13.2 us (5%)
  other arithmetic  12.8 us (4%)
  starting transfers between devices  6.71 us (2%)
  loops' own time  5.6 us (2%)
    all_gather x1, waiting for transfers between devices, sent_together(): lax.all_gather(both, axis, axis=dim, tiled=True)  98.9 us
    dot_general x8, matrix products, update(): jnp.einsum('cqhk,kv->cqhv', weights.astype(jnp.bfloat16), value_block, pr...  42.1 us
    dot_general x8, matrix products, update(): jnp.einsum('qhcd,kcd->cqhk', queries, key_block.reshape(key_block.shape[0...  36.2 us
    all_to_all x1, waiting for transfers between devices, copy_for_each(): lax.all_to_all(jnp.broadcast_to(x[None], (count, *x.shape)), axis, 0, 0,...  24.6 us
    all_to_all x1, blocking collectives, local(): lax.all_to_all(jnp.stack(jnp.split(normed, lax.axis_size('tp'), axis=0)),...  13.2 us
    reduce_sum x8, other arithmetic, update(): running_sum = shrink * running_sum + jnp.sum(weights, axis=-1)  11 us
    dynamic_slice x8, local copies, waits for them, and re-layouts, one_span(): lax.dynamic_slice_in_dim(key_piece, span_index * fold_span, fold_span, 0)  8.65 us
    all_to_all x1, starting transfers between devices, copy_for_each(): lax.all_to_all(jnp.broadcast_to(x[None], (count, *x.shape)), axis, 0, 0,...  6.7 us
  transfers between devices with their start and end apart: 2, of which 2 were waited for; matrix products, arithmetic and copies ran while one was open for 1% of the time, Pallas kernels for 0%

profile of v1, /device:TPU:1, one launch (start us, length us, event | category | flops | bytes accessed | tf_op | source)
XLA Modules:
  0.0 288.4 jit_solution(2157014576865928422)
XLA Ops:
  6.5 2.5 broadcast_in_dim.11
  9.1 6.7 %all-to-all-start = ((bf16[8,64,2048]{2,1,0:T(8,128)(2,1)}), bf16[8,64,2048]{2,1,0:T(8,128)(2,1)S(1)}, u32[]{:S(2)}, u32[]{:S(2)}) async-start(bf16[8,64,2048]{2,1,0:T(8,128)(2,1)} %broadcast_in_dim.11), calls=%async_computation | async-start | bytes 4194304 | tf_op jit(solution)/shard_map/all_to_all | solution.py:22
  15.8 0.0 all-gather.2.cloned.1.call-start
  15.8 0.3 multiply_cosine_fusion
  16.1 1.3 constant_dynamic-slice_fusion.1
  17.4 24.6 %all-to-all-done = bf16[8,64,2048]{2,1,0:T(8,128)(2,1)S(1)} async-done(((bf16[8,64,2048]{2,1,0:T(8,128)(2,1)}), bf16[8,64,2048]{2,1,0:T(8,128)(2,1)S(1)}, u32[]{:S(2)}, u32[]{:S(2)}) %all-to-all-start) | async-done | bytes 2097184 | tf_op jit(solution)/shard_map/all_to_all | solution.py:22
  42.0 2.1 fusion.24
  44.2 0.7 pad_maximum_fusion
  44.9 0.0 all-gather.2.cloned.1.call-update
  45.7 98.9 %all-gather.2.cloned.1.call-done = bf16[16384,256]{0,1:T(8,128)(2,1)} async-done(((bf16[512,256]{0,1:T(8,128)(2,1)}), bf16[16384,256]{0,1:T(8,128)(2,1)}) %all-gather.2.cloned.1.call-update) | async-done | bytes 8388624 | tf_op jit(solution)/shard_map/all_gather | solution.py:35
  144.6 5.8 %fusion.33 = (bf16[16384,128]{0,1:T(8,128)(2,1)}, bf16[16384,128]{0,1:T(8,128)(2,1)}) fusion(bf16[16384,256]{0,1:T(8,128)(2,1)} %all-gather.2.cloned.1.call-done), kind=kLoop, calls=%fused_computation.70 | loop fusion | bytes 16777216 | tf_op jit(solution)/shard_map/split | solution.py:35
  150.4 113.6 %while.15 = (s32[]{:T(128)}, f32[2,512,1]{1,0,2:T(2,128)S(1)}, f32[2,512,1]{1,0,2:T(2,128)S(1)}, f32[2,512,1,128]{3,1,0,2:T(8,128)S(1)}, s32[8]{0:T(128)S(1)}, /...) while((s32[]{:T(128)}, f32[2,512,1]{1,0,2:T(2,128)S(1)}, ...), condition=%wide.region_3.4_spmd.clone, body=%wide.region_0.3_spmd.clone.sunk | while | flops 822482944 | bytes 62062812 | solution.py:115
  150.4 0.6 dynamic_slice.33
  151.7 1.1 constant_dynamic-slice_fusion.4
  152.8 4.5 %bitcast_reduce_fusion.2 = (f32[2,512]{1,0:T(2,128)S(1)}, f32[2,2048,512]{2,1,0:T(8,128)}) fusion(bf16[2048,2,64]{0,2,1:T(8,128)(2,1)S(1)} %bitcast.127, bf16[512,1,2,64]{0,3,2,1:T(8,128)(2,1)S(1)} %get-tuple-element.216), kind=kOutput, calls=%fused_computation.1.clone.1 | convolution fusion | flops 272628736 | bytes 9048064 | tf_op jit(solution)/shard_map/while/body/eval_jaxpr/qhcd,kcd->cqhk/dot_general | solution.py:82
  157.3 5.3 %fusion.51 = f32[2,512,1,128]{3,1,0,2:T(8,128)S(1)} fusion(f32[2,2048,512]{2,1,0:T(8,128)} %get-tuple-element.184, f32[2,512]{1,0:T(2,128)S(1)} %bitcast.129, f32[2,512,1,128]{3,1,0,2:T(8,128)S(1)} %get-tuple-element.201, bf16[16384,128]{0,1:T(8,128)(2,1)} %get-tuple-element.217, s32[]{:T(128)S(6)} %select_n.17, ...), kind=kOutput, calls=%fused_computation.7.clone.1 | convolution fusion | flops 543555584 | bytes 9969669 | tf_op jit(solution)/shard_map/while/body/eval_jaxpr/cqhk,kv->cqhv/dot_general | solution.py:94
  162.6 0.6 copy-done
  163.2 1.4 fusion.50
  164.6 0.6 dynamic_slice.33
  165.9 1.1 constant_dynamic-slice_fusion.4
  167.0 4.5 %bitcast_reduce_fusion.2 = (f32[2,512]{1,0:T(2,128)S(1)}, f32[2,2048,512]{2,1,0:T(8,128)}) fusion(bf16[2048,2,64]{0,2,1:T(8,128)(2,1)S(1)} %bitcast.127, bf16[512,1,2,64]{0,3,2,1:T(8,128)(2,1)S(1)} %get-tuple-element.216), kind=kOutput, calls=%fused_computation.1.clone.1 | convolution fusion | flops 272628736 | bytes 9048064 | tf_op jit(solution)/shard_map/while/body/eval_jaxpr/qhcd,kcd->cqhk/dot_general | solution.py:82
  171.5 5.3 %fusion.51 = f32[2,512,1,128]{3,1,0,2:T(8,128)S(1)} fusion(f32[2,2048,512]{2,1,0:T(8,128)} %get-tuple-element.184, f32[2,512]{1,0:T(2,128)S(1)} %bitcast.129, f32[2,512,1,128]{3,1,0,2:T(8,128)S(1)} %get-tuple-element.201, bf16[16384,128]{0,1:T(8,128)(2,1)} %get-tuple-element.217, s32[]{:T(128)S(6)} %select_n.17, ...), kind=kOutput, calls=%fused_computation.7.clone.1 | convolution fusion | flops 543555584 | bytes 9969669 | tf_op jit(solution)/shard_map/while/body/eval_jaxpr/cqhk,kv->cqhv/dot_general | solution.py:94
  176.8 0.6 copy-done
  177.4 1.4 fusion.50
  178.9 0.6 dynamic_slice.33
  180.1 1.1 constant_dynamic-slice_fusion.4
  181.2 4.5 %bitcast_reduce_fusion.2 = (f32[2,512]{1,0:T(2,128)S(1)}, f32[2,2048,512]{2,1,0:T(8,128)}) fusion(bf16[2048,2,64]{0,2,1:T(8,128)(2,1)S(1)} %bitcast.127, bf16[512,1,2,64]{0,3,2,1:T(8,128)(2,1)S(1)} %get-tuple-element.216), kind=kOutput, calls=%fused_computation.1.clone.1 | convolution fusion | flops 272628736 | bytes 9048064 | tf_op jit(solution)/shard_map/while/body/eval_jaxpr/qhcd,kcd->cqhk/dot_general | solution.py:82
  185.7 5.3 %fusion.51 = f32[2,512,1,128]{3,1,0,2:T(8,128)S(1)} fusion(f32[2,2048,512]{2,1,0:T(8,128)} %get-tuple-element.184, f32[2,512]{1,0:T(2,128)S(1)} %bitcast.129, f32[2,512,1,128]{3,1,0,2:T(8,128)S(1)} %get-tuple-element.201, bf16[16384,128]{0,1:T(8,128)(2,1)} %get-tuple-element.217, s32[]{:T(128)S(6)} %select_n.17, ...), kind=kOutput, calls=%fused_computation.7.clone.1 | convolution fusion | flops 543555584 | bytes 9969669 | tf_op jit(solution)/shard_map/while/body/eval_jaxpr/cqhk,kv->cqhv/dot_general | solution.py:94
  191.0 0.6 copy-done
  191.6 1.4 fusion.50
  193.1 0.6 dynamic_slice.33
  194.3 1.1 constant_dynamic-slice_fusion.4
  195.4 4.5 %bitcast_reduce_fusion.2 = (f32[2,512]{1,0:T(2,128)S(1)}, f32[2,2048,512]{2,1,0:T(8,128)}) fusion(bf16[2048,2,64]{0,2,1:T(8,128)(2,1)S(1)} %bitcast.127, bf16[512,1,2,64]{0,3,2,1:T(8,128)(2,1)S(1)} %get-tuple-element.216), kind=kOutput, calls=%fused_computation.1.clone.1 | convolution fusion | flops 272628736 | bytes 9048064 | tf_op jit(solution)/shard_map/while/body/eval_jaxpr/qhcd,kcd->cqhk/dot_general | solution.py:82
  199.9 5.3 %fusion.51 = f32[2,512,1,128]{3,1,0,2:T(8,128)S(1)} fusion(f32[2,2048,512]{2,1,0:T(8,128)} %get-tuple-element.184, f32[2,512]{1,0:T(2,128)S(1)} %bitcast.129, f32[2,512,1,128]{3,1,0,2:T(8,128)S(1)} %get-tuple-element.201, bf16[16384,128]{0,1:T(8,128)(2,1)} %get-tuple-element.217, s32[]{:T(128)S(6)} %select_n.17, ...), kind=kOutput, calls=%fused_computation.7.clone.1 | convolution fusion | flops 543555584 | bytes 9969669 | tf_op jit(solution)/shard_map/while/body/eval_jaxpr/cqhk,kv->cqhv/dot_general | solution.py:94
  205.2 0.6 copy-done
  205.8 1.4 fusion.50
  207.3 0.6 dynamic_slice.33
  208.5 1.1 constant_dynamic-slice_fusion.4
  209.6 4.5 %bitcast_reduce_fusion.2 = (f32[2,512]{1,0:T(2,128)S(1)}, f32[2,2048,512]{2,1,0:T(8,128)}) fusion(bf16[2048,2,64]{0,2,1:T(8,128)(2,1)S(1)} %bitcast.127, bf16[512,1,2,64]{0,3,2,1:T(8,128)(2,1)S(1)} %get-tuple-element.216), kind=kOutput, calls=%fused_computation.1.clone.1 | convolution fusion | flops 272628736 | bytes 9048064 | tf_op jit(solution)/shard_map/while/body/eval_jaxpr/qhcd,kcd->cqhk/dot_general | solution.py:82
  214.1 5.3 %fusion.51 = f32[2,512,1,128]{3,1,0,2:T(8,128)S(1)} fusion(f32[2,2048,512]{2,1,0:T(8,128)} %get-tuple-element.184, f32[2,512]{1,0:T(2,128)S(1)} %bitcast.129, f32[2,512,1,128]{3,1,0,2:T(8,128)S(1)} %get-tuple-element.201, bf16[16384,128]{0,1:T(8,128)(2,1)} %get-tuple-element.217, s32[]{:T(128)S(6)} %select_n.17, ...), kind=kOutput, calls=%fused_computation.7.clone.1 | convolution fusion | flops 543555584 | bytes 9969669 | tf_op jit(solution)/shard_map/while/body/eval_jaxpr/cqhk,kv->cqhv/dot_general | solution.py:94
  219.4 0.6 copy-done
  220.1 1.4 fusion.50
  221.5 0.6 dynamic_slice.33
  222.7 1.1 constant_dynamic-slice_fusion.4
  223.8 4.5 %bitcast_reduce_fusion.2 = (f32[2,512]{1,0:T(2,128)S(1)}, f32[2,2048,512]{2,1,0:T(8,128)}) fusion(bf16[2048,2,64]{0,2,1:T(8,128)(2,1)S(1)} %bitcast.127, bf16[512,1,2,64]{0,3,2,1:T(8,128)(2,1)S(1)} %get-tuple-element.216), kind=kOutput, calls=%fused_computation.1.clone.1 | convolution fusion | flops 272628736 | bytes 9048064 | tf_op jit(solution)/shard_map/while/body/eval_jaxpr/qhcd,kcd->cqhk/dot_general | solution.py:82
  228.4 5.3 %fusion.51 = f32[2,512,1,128]{3,1,0,2:T(8,128)S(1)} fusion(f32[2,2048,512]{2,1,0:T(8,128)} %get-tuple-element.184, f32[2,512]{1,0:T(2,128)S(1)} %bitcast.129, f32[2,512,1,128]{3,1,0,2:T(8,128)S(1)} %get-tuple-element.201, bf16[16384,128]{0,1:T(8,128)(2,1)} %get-tuple-element.217, s32[]{:T(128)S(6)} %select_n.17, ...), kind=kOutput, calls=%fused_computation.7.clone.1 | convolution fusion | flops 543555584 | bytes 9969669 | tf_op jit(solution)/shard_map/while/body/eval_jaxpr/cqhk,kv->cqhv/dot_general | solution.py:94
  233.6 0.6 copy-done
  234.3 1.4 fusion.50
  235.7 0.6 dynamic_slice.33
  236.9 1.1 constant_dynamic-slice_fusion.4
  238.0 4.5 %bitcast_reduce_fusion.2 = (f32[2,512]{1,0:T(2,128)S(1)}, f32[2,2048,512]{2,1,0:T(8,128)}) fusion(bf16[2048,2,64]{0,2,1:T(8,128)(2,1)S(1)} %bitcast.127, bf16[512,1,2,64]{0,3,2,1:T(8,128)(2,1)S(1)} %get-tuple-element.216), kind=kOutput, calls=%fused_computation.1.clone.1 | convolution fusion | flops 272628736 | bytes 9048064 | tf_op jit(solution)/shard_map/while/body/eval_jaxpr/qhcd,kcd->cqhk/dot_general | solution.py:82
  242.6 5.3 %fusion.51 = f32[2,512,1,128]{3,1,0,2:T(8,128)S(1)} fusion(f32[2,2048,512]{2,1,0:T(8,128)} %get-tuple-element.184, f32[2,512]{1,0:T(2,128)S(1)} %bitcast.129, f32[2,512,1,128]{3,1,0,2:T(8,128)S(1)} %get-tuple-element.201, bf16[16384,128]{0,1:T(8,128)(2,1)} %get-tuple-element.217, s32[]{:T(128)S(6)} %select_n.17, ...), kind=kOutput, calls=%fused_computation.7.clone.1 | convolution fusion | flops 543555584 | bytes 9969669 | tf_op jit(solution)/shard_map/while/body/eval_jaxpr/cqhk,kv->cqhv/dot_general | solution.py:94
  247.8 0.6 copy-done
  248.5 1.4 fusion.50
  249.9 0.6 dynamic_slice.33
  251.1 1.1 constant_dynamic-slice_fusion.4
  252.2 4.5 %bitcast_reduce_fusion.2 = (f32[2,512]{1,0:T(2,128)S(1)}, f32[2,2048,512]{2,1,0:T(8,128)}) fusion(bf16[2048,2,64]{0,2,1:T(8,128)(2,1)S(1)} %bitcast.127, bf16[512,1,2,64]{0,3,2,1:T(8,128)(2,1)S(1)} %get-tuple-element.216), kind=kOutput, calls=%fused_computation.1.clone.1 | convolution fusion | flops 272628736 | bytes 9048064 | tf_op jit(solution)/shard_map/while/body/eval_jaxpr/qhcd,kcd->cqhk/dot_general | solution.py:82
  256.8 5.3 %fusion.51 = f32[2,512,1,128]{3,1,0,2:T(8,128)S(1)} fusion(f32[2,2048,512]{2,1,0:T(8,128)} %get-tuple-element.184, f32[2,512]{1,0:T(2,128)S(1)} %bitcast.129, f32[2,512,1,128]{3,1,0,2:T(8,128)S(1)} %get-tuple-element.201, bf16[16384,128]{0,1:T(8,128)(2,1)} %get-tuple-element.217, s32[]{:T(128)S(6)} %select_n.17, ...), kind=kOutput, calls=%fused_computation.7.clone.1 | convolution fusion | flops 543555584 | bytes 9969669 | tf_op jit(solution)/shard_map/while/body/eval_jaxpr/cqhk,kv->cqhv/dot_general | solution.py:94
  262.0 0.6 copy-done
  262.7 1.4 fusion.50
  264.1 0.3 multiply_reduce_fusion
  264.4 0.1 multiply_convert_fusion
  264.7 13.2 %all_to_all.10 = bf16[8,64,128]{2,1,0:T(8,128)(2,1)S(1)} all-to-all(bf16[8,64,128]{2,1,0:T(8,128)(2,1)S(1)} %constant_dynamic-update-slice_fusion), channel_id=1, replica_groups=mesh['sp'=32,'tp'=8] {'tp'}, dimensions={0} | all-to-all | bytes 262144 | tf_op jit(solution)/shard_map/all_to_all | solution.py:126
  277.9 3.7 %convolution_convert_fusion = bf16[64,2048]{1,0:T(8,128)(2,1)} fusion(bf16[1024,2048]{1,0:T(8,128)(2,1)} %param.13, bf16[8,64,128]{2,1,0:T(8,128)(2,1)S(1)} %all_to_all.10), kind=kOutput, calls=%fused_computation.22 | convolution fusion | flops 268566528 | bytes 4587520 | tf_op jit(solution)/shard_map/dot_general | solution.py:129
  (56 shorter events, 0.6 us)
Async XLA Ops:
  9.1 32.9 %all-to-all-start = ((bf16[8,64,2048]{2,1,0:T(8,128)(2,1)}), bf16[8,64,2048]{2,1,0:T(8,128)(2,1)S(1)}, u32[]{:S(2)}, u32[]{:S(2)}) async-start(bf16[8,64,2048]{2,1,0:T(8,128)(2,1)} %broadcast_in_dim.11), calls=%async_computation | async-start | bytes 4194304 | tf_op jit(solution)/shard_map/all_to_all | solution.py:22
  15.8 128.8 %all-gather.2.cloned.1.call-start = ((), (), s32[]{:S(2)}) async-start(), calls=%async_computation.2 | async-start | bytes 8650752 | tf_op jit(solution)/shard_map/all_gather | solution.py:35
  150.4 114.0 %copy-start.1 = (f32[128]{0:T(128)S(1)}, f32[128]{0:T(128)}, u32[]{:S(2)}) copy-start(f32[128]{0:T(128)} %param.14) | copy-start | bytes 1540
  157.3 5.9 %copy-start = (f32[2,2048,512]{2,1,0:T(8,128)S(1)}, f32[2,2048,512]{2,1,0:T(8,128)}, u32[]{:S(2)}) copy-start(f32[2,2048,512]{2,1,0:T(8,128)} %get-tuple-element.184) | copy-start | bytes 25165828 | tf_op jit(solution)/shard_map/while
  171.5 5.9 %copy-start = (f32[2,2048,512]{2,1,0:T(8,128)S(1)}, f32[2,2048,512]{2,1,0:T(8,128)}, u32[]{:S(2)}) copy-start(f32[2,2048,512]{2,1,0:T(8,128)} %get-tuple-element.184) | copy-start | bytes 25165828 | tf_op jit(solution)/shard_map/while
  185.7 5.9 %copy-start = (f32[2,2048,512]{2,1,0:T(8,128)S(1)}, f32[2,2048,512]{2,1,0:T(8,128)}, u32[]{:S(2)}) copy-start(f32[2,2048,512]{2,1,0:T(8,128)} %get-tuple-element.184) | copy-start | bytes 25165828 | tf_op jit(solution)/shard_map/while
  199.9 5.9 %copy-start = (f32[2,2048,512]{2,1,0:T(8,128)S(1)}, f32[2,2048,512]{2,1,0:T(8,128)}, u32[]{:S(2)}) copy-start(f32[2,2048,512]{2,1,0:T(8,128)} %get-tuple-element.184) | copy-start | bytes 25165828 | tf_op jit(solution)/shard_map/while
  214.1 5.9 %copy-start = (f32[2,2048,512]{2,1,0:T(8,128)S(1)}, f32[2,2048,512]{2,1,0:T(8,128)}, u32[]{:S(2)}) copy-start(f32[2,2048,512]{2,1,0:T(8,128)} %get-tuple-element.184) | copy-start | bytes 25165828 | tf_op jit(solution)/shard_map/while
  228.3 5.9 %copy-start = (f32[2,2048,512]{2,1,0:T(8,128)S(1)}, f32[2,2048,512]{2,1,0:T(8,128)}, u32[]{:S(2)}) copy-start(f32[2,2048,512]{2,1,0:T(8,128)} %get-tuple-element.184) | copy-start | bytes 25165828 | tf_op jit(solution)/shard_map/while
  242.5 5.9 %copy-start = (f32[2,2048,512]{2,1,0:T(8,128)S(1)}, f32[2,2048,512]{2,1,0:T(8,128)}, u32[]{:S(2)}) copy-start(f32[2,2048,512]{2,1,0:T(8,128)} %get-tuple-element.184) | copy-start | bytes 25165828 | tf_op jit(solution)/shard_map/while
  256.8 5.9 %copy-start = (f32[2,2048,512]{2,1,0:T(8,128)S(1)}, f32[2,2048,512]{2,1,0:T(8,128)}, u32[]{:S(2)}) copy-start(f32[2,2048,512]{2,1,0:T(8,128)} %get-tuple-element.184) | copy-start | bytes 25165828 | tf_op jit(solution)/shard_map/while
Sparse Core Ops, SparseCore 0:
  45.1 99.4 all-gather.1
